TPU v7x, 32 devices: a whole 2x2x4 slice. The times are simulated.
32 devices in a mesh: rep: 2 (over x), fs: 8 (over z, y), tp: 2 (over core).
Axes of the slice: x: 2, y: 2, z: 4, core: 2. Of those that a mesh axis runs over, the one named last changes fastest.
Arguments:
- stream: bfloat16 [4096, 2048], P(('rep', 'fs'), 'tp'), may hold values from -6 to 6
- norm_gains: float32 [6, 2048], replicated, may hold values from 0.1 to 1.9
- w_gate: bfloat16 [2048, 5632], P('fs', 'tp'), may hold values from -0.125 to 0.125
- w_up: bfloat16 [2048, 5632], P('fs', 'tp'), may hold values from -0.125 to 0.125
- w_down: bfloat16 [5632, 2048], P('tp', 'fs'), may hold values from -0.109375 to 0.109375
- w_inner: bfloat16 [2048, 1024], P('fs', 'tp'), may hold values from -0.125 to 0.125
- w_bgate: bfloat16 [2048, 1024], P('fs', 'tp'), may hold values from -0.125 to 0.125
- w_cgate: bfloat16 [2048, 1024], P('fs', 'tp'), may hold values from -0.125 to 0.125
- conv_taps: float32 [3, 1024], P(None, 'tp'), may hold values from -3.5 to 3.5
- w_out: bfloat16 [1024, 2048], P('tp', 'fs'), may hold values from -0.25 to 0.25
Outputs:
- mixed: bfloat16 [4096, 2048], P(('rep', 'fs'), 'tp')
All inputs are finite; a program needn't handle non-finite values.
Results may differ from a plain program's by a relative error of at most 0.02.
Values may be sent and summed in bfloat16 or wider, within the bound.
A program may use at most 128 MiB of HBM per device.

v0:
```python
import jax
import jax.numpy as jnp
from jax import lax
from jax.sharding import PartitionSpec as P

TAPS = 3
EPSILON = 1e-06


def from_behind(x, axis, by):
    count = lax.axis_size(axis)
    pairs = [(i, i + by) for i in range(count) if 0 <= i + by < count]
    return lax.ppermute(x, axis, pairs)


def shards(stream, norm_gains, w_gate, w_up, w_down, w_inner, w_bgate, w_cgate, conv_taps, w_out):
    tp_index = lax.axis_index("tp")
    local_width = stream.shape[1]
    model_width = local_width * lax.axis_size("tp")

    def own_gain(row):
        return lax.dynamic_slice_in_dim(norm_gains[row], tp_index * local_width, local_width, 0)

    def gathered_norm(current, row):
        gathered = lax.all_gather(current, "tp", axis=1, tiled=True)
        values = gathered.astype(jnp.float32)
        scaled = values * lax.rsqrt(jnp.mean(values * values, axis=1, keepdims=True) + EPSILON)
        return (scaled * norm_gains[row]).astype(jnp.bfloat16)

    def settle(current, partials, row, weight):
        branch_sum = lax.psum_scatter(
            partials.astype(jnp.bfloat16), "tp", scatter_dimension=1, tiled=True
        ).astype(jnp.float32)
        squares = lax.psum(jnp.sum(branch_sum * branch_sum, axis=1), "tp")
        scaled = branch_sum * lax.rsqrt(squares / model_width + EPSILON)[:, None]
        return (current.astype(jnp.float32) + weight * (scaled * own_gain(row))).astype(
            jnp.bfloat16
        )

    gate_whole, up_whole, down_whole = (
        lax.all_gather(w_gate, "fs", axis=0, tiled=True),
        lax.all_gather(w_up, "fs", axis=0, tiled=True),
        lax.all_gather(w_down, "fs", axis=1, tiled=True),
    )

    def feed_forward(current, row_in, row_out):
        normed = gathered_norm(current, row_in)
        gate_vals = jnp.dot(normed, gate_whole, preferred_element_type=jnp.float32)
        upward = jnp.dot(normed, up_whole, preferred_element_type=jnp.float32)
        hidden = (jax.nn.silu(gate_vals) * upward).astype(jnp.bfloat16)
        partials = jnp.dot(hidden, down_whole, preferred_element_type=jnp.float32)
        return settle(current, partials, row_out, 0.5)

    first = feed_forward(stream, 0, 1)
    normed_mix = gathered_norm(first, 2)
    local_rows = normed_mix.shape[0]

    def fold_rows(block_rows):
        return jnp.dot(normed_mix, block_rows, preferred_element_type=jnp.float32)

    inner = fold_rows(lax.all_gather(w_inner, "fs", axis=0, tiled=True))
    bgate = fold_rows(lax.all_gather(w_bgate, "fs", axis=0, tiled=True))
    cgate = fold_rows(lax.all_gather(w_cgate, "fs", axis=0, tiled=True))
    conv_input = cgate * inner
    earlier = from_behind(conv_input[local_rows - (TAPS - 1) :], "fs", 1)
    padded = jnp.concatenate([earlier, conv_input], axis=0)
    conv = conv_taps[0] * padded[0:local_rows]
    for tap in range(1, TAPS):
        conv = conv + conv_taps[tap] * padded[tap : tap + local_rows]
    gated = (bgate * conv).astype(jnp.bfloat16)
    mix_partials = jnp.dot(
        gated, lax.all_gather(w_out, "fs", axis=1, tiled=True), preferred_element_type=jnp.float32
    )
    second = settle(first, mix_partials, 3, 1.0)
    return feed_forward(second, 4, 5)


def solution(mesh):
    return jax.shard_map(
        shards,
        mesh=mesh,
        in_specs=(
            P(("rep", "fs"), "tp"),
            P(),
            P("fs", "tp"),
            P("fs", "tp"),
            P("tp", "fs"),
            P("fs", "tp"),
            P("fs", "tp"),
            P("fs", "tp"),
            P(None, "tp"),
            P("tp", "fs"),
        ),
        out_specs=P(("rep", "fs"), "tp"),
        check_vma=False,
    )
```

profile of v0, /device:TPU:0, one launch (start us, length us, event | category | flops | bytes accessed | tf_op | source)
XLA Modules:
  0.0 832.3 jit_solution(3071890299738791454)
XLA Ops:
  6.5 0.0 all-gather.11.cloned.1.call-start
  6.5 0.7 all-gather.11.cloned.1.call-update
  7.3 0.0 all-gather.13.cloned.1.call-start
  7.3 0.7 all-gather.13.cloned.1.call-update
  8.0 0.0 all-gather.15.cloned.1.call-start
  8.1 0.7 all-gather.15.cloned.1.call-update
  8.8 0.0 all-gather.17.cloned.1.call-start
  8.8 0.5 all-gather.17.cloned.1.call-update
  9.3 0.0 reduce-scatter.4.cloned.1.call-start
  9.4 11.2 %all-gather.11.cloned.1.call-done = bf16[256,2048]{1,0:T(8,128)(2,1)} async-done(((bf16[256,1024]{1,0:T(8,128)(2,1)}), bf16[256,2048]{1,0:T(8,128)(2,1)}) %all-gather.11.cloned.1.call-update) | async-done | bytes 1048592 | tf_op jit(solution)/shard_map/all_gather | solution.py:25
  20.7 1.5 fusion.2
  22.2 165.2 %all-gather.13.cloned.1.call-done = bf16[2048,2816]{1,0:T(8,128)(2,1)} async-done(((bf16[256,2816]{1,0:T(8,128)(2,1)}), bf16[2048,2816]{1,0:T(8,128)(2,1)}) %all-gather.13.cloned.1.call-update) | async-done | bytes 11534352 | tf_op jit(solution)/shard_map/all_gather | solution.py:41
  187.4 9.5 %fusion.38 = f32[256,2816]{1,0:T(8,128)} fusion(bf16[2048,2816]{1,0:T(8,128)(2,1)} %all-gather.13.cloned.1.call-done, bf16[256,2048]{1,0:T(8,128)(2,1)} %all-gather.11.cloned.1.call-done, f32[2048]{0:T(1024)S(1)} %bitcast.27, f32[256]{0:T(256)S(1)} %add_rsqrt_fusion.5), kind=kOutput, calls=%fused_computation.54 | convolution fusion | flops 2954887168 | bytes 15475712 | tf_op jit(solution)/shard_map/dot_general | solution.py:48
  196.9 154.2 %all-gather.15.cloned.1.call-done = bf16[2048,2816]{1,0:T(8,128)(2,1)} async-done(((bf16[256,2816]{1,0:T(8,128)(2,1)}), bf16[2048,2816]{1,0:T(8,128)(2,1)}) %all-gather.15.cloned.1.call-update) | async-done | bytes 11534352 | tf_op jit(solution)/shard_map/all_gather | solution.py:42
  351.1 163.4 %all-gather.17.cloned.1.call-done = bf16[2816,2048]{1,0:T(8,128)(2,1)} async-done(((bf16[2816,256]{1,0:T(8,128)(2,1)}), bf16[2816,2048]{1,0:T(8,128)(2,1)}) %all-gather.17.cloned.1.call-update) | async-done | bytes 11534352 | tf_op jit(solution)/shard_map/all_gather | solution.py:43
  514.5 15.6 %convolution_convert_fusion.2 = bf16[256,2048]{1,0:T(8,128)(2,1)} fusion(bf16[2816,2048]{1,0:T(8,128)(2,1)} %all-gather.17.cloned.1.call-done, bf16[2048,2816]{1,0:T(8,128)(2,1)} %all-gather.15.cloned.1.call-done, f32[256,2816]{1,0:T(8,128)} %fusion.38, bf16[256,2048]{1,0:T(8,128)(2,1)S(1)} %copy-done.4, f32[2048]{0:T(1024)S(1)} %bitcast.28, ...), kind=kOutput, calls=%fused_computation.12 | convolution fusion | flops 5912526848 | bytes 28058624 | tf_op jit(solution)/shard_map/dot_general | solution.py:51
  530.1 0.0 reduce-scatter.4.cloned.1.call-update
  530.2 0.0 all-gather.19.cloned.1.call-start
  530.2 6.6 reduce-scatter.4.cloned.1.call-done
  536.9 1.2 fusion.11
  538.1 2.5 psum.21
  540.6 0.0 copy-done.2
  540.6 2.1 fusion.15
  542.7 0.0 all-gather.19.cloned.1.call-update
  542.7 0.0 all-gather.23.cloned.1.call-start
  542.8 0.7 all-gather.23.cloned.1.call-update
  543.5 0.0 all-gather.25.cloned.1.call-start
  543.5 0.7 all-gather.25.cloned.1.call-update
  544.2 0.0 all-gather.21.cloned.1.call-start
  544.3 0.7 all-gather.21.cloned.1.call-update
  545.0 0.0 all-gather.27.cloned.1.call-start
  545.0 0.5 all-gather.27.cloned.1.call-update
  545.6 0.0 reduce-scatter.6.cloned.1.call-start
  545.6 7.5 all-gather.19.cloned.1.call-done
  553.1 1.5 fusion.5
  554.6 50.9 %all-gather.23.cloned.1.call-done = bf16[2048,512]{1,0:T(8,128)(2,1)} async-done(((bf16[256,512]{1,0:T(8,128)(2,1)}), bf16[2048,512]{1,0:T(8,128)(2,1)}) %all-gather.23.cloned.1.call-update) | async-done | bytes 2097168 | tf_op jit(solution)/shard_map/all_gather | solution.py:63
  605.5 2.7 fusion.48
  608.3 0.0 copy-start.7
  608.3 47.0 %all-gather.25.cloned.1.call-done = bf16[2048,512]{1,0:T(8,128)(2,1)} async-done(((bf16[256,512]{1,0:T(8,128)(2,1)}), bf16[2048,512]{1,0:T(8,128)(2,1)}) %all-gather.25.cloned.1.call-update) | async-done | bytes 2097168 | tf_op jit(solution)/shard_map/all_gather | solution.py:61
  655.3 2.3 convolution_multiply_fusion.2
  657.6 2.5 collective-permute-start
  660.1 44.9 %all-gather.21.cloned.1.call-done = bf16[2048,512]{1,0:T(8,128)(2,1)} async-done(((bf16[256,512]{1,0:T(8,128)(2,1)}), bf16[2048,512]{1,0:T(8,128)(2,1)}) %all-gather.21.cloned.1.call-update) | async-done | bytes 2097168 | tf_op jit(solution)/shard_map/all_gather | solution.py:62
  705.1 50.8 %all-gather.27.cloned.1.call-done = bf16[512,2048]{1,0:T(8,128)(2,1)} async-done(((bf16[512,256]{1,0:T(8,128)(2,1)}), bf16[512,2048]{1,0:T(8,128)(2,1)}) %all-gather.27.cloned.1.call-update) | async-done | bytes 2097168 | tf_op jit(solution)/shard_map/all_gather | solution.py:72
  755.9 0.0 collective-permute-done
  755.9 4.7 convolution_convert_fusion.1
  760.6 0.0 reduce-scatter.6.cloned.1.call-update
  760.6 0.0 all-gather.29.cloned.1.call-start
  760.6 6.7 reduce-scatter.6.cloned.1.call-done
  767.3 1.2 fusion.16
  768.5 2.5 psum.22
  771.0 0.0 copy-done
  771.0 2.1 fusion.19
  773.1 0.0 all-gather.29.cloned.1.call-update
  773.1 0.2 reduce-scatter.8.cloned.1.call-start
  773.4 10.1 %all-gather.29.cloned.1.call-done = bf16[256,2048]{1,0:T(8,128)(2,1)} async-done(((bf16[256,1024]{1,0:T(8,128)(2,1)}), bf16[256,2048]{1,0:T(8,128)(2,1)}) %all-gather.29.cloned.1.call-update) | async-done | bytes 1048592 | tf_op jit(solution)/shard_map/all_gather | solution.py:25
  783.5 1.5 fusion.8
  785.0 0.0 copy-start.5
  785.0 9.5 %fusion.34 = f32[256,2816]{1,0:T(8,128)} fusion(bf16[2048,2816]{1,0:T(8,128)(2,1)} %all-gather.13.cloned.1.call-done, bf16[256,2048]{1,0:T(8,128)(2,1)} %all-gather.29.cloned.1.call-done, f32[2048]{0:T(1024)S(1)} %bitcast.22, f32[256]{0:T(256)S(1)} %add_rsqrt_fusion.1), kind=kOutput, calls=%fused_computation.53 | convolution fusion | flops 2954887168 | bytes 15475712 | tf_op jit(solution)/shard_map/dot_general | solution.py:48
  794.5 15.7 %convolution_convert_fusion = bf16[256,2048]{1,0:T(8,128)(2,1)} fusion(bf16[2816,2048]{1,0:T(8,128)(2,1)} %all-gather.17.cloned.1.call-done, bf16[2048,2816]{1,0:T(8,128)(2,1)} %all-gather.15.cloned.1.call-done, f32[256,2816]{1,0:T(8,128)} %fusion.34, bf16[256,2048]{1,0:T(8,128)(2,1)S(1)} %copy-done.5, f32[2048]{0:T(1024)S(1)} %bitcast.23, ...), kind=kOutput, calls=%fused_computation.10 | convolution fusion | flops 5912526848 | bytes 28058624 | tf_op jit(solution)/shard_map/dot_general | solution.py:51
  810.2 0.0 reduce-scatter.8.cloned.1.call-update
  810.3 9.7 %reduce-scatter.8.cloned.1.call-done = bf16[256,1024]{1,0:T(8,128)(2,1)} async-done(((bf16[256,2048]{1,0:T(8,128)(2,1)}), bf16[256,1024]{1,0:T(8,128)(2,1)}) %reduce-scatter.8.cloned.1.call-update) | async-done | bytes 524304 | tf_op jit(solution)/shard_map/reduce_scatter | solution.py:31
  820.0 1.2 fusion.20
  821.2 2.5 psum.23
  823.7 2.1 fusion.24
  (24 shorter events, 0.1 us)
Async XLA Ops:
  6.5 14.1 %all-gather.11.cloned.1.call-start = ((), (), s32[]{:S(2)}) async-start(), calls=%async_computation.3 | async-start | bytes 1572864 | tf_op jit(solution)/shard_map/all_gather | solution.py:25
  7.3 2.1 copy-start.6
  7.3 180.1 %all-gather.13.cloned.1.call-start = ((), (), s32[]{:S(2)}) async-start(), calls=%async_computation.4 | async-start | bytes 12976128 | tf_op jit(solution)/shard_map/all_gather | solution.py:41
  8.0 343.1 %all-gather.15.cloned.1.call-start = ((), (), s32[]{:S(2)}) async-start(), calls=%async_computation.5 | async-start | bytes 12976128 | tf_op jit(solution)/shard_map/all_gather | solution.py:42
  8.8 505.8 %all-gather.17.cloned.1.call-start = ((), (), s32[]{:S(2)}) async-start(), calls=%async_computation.6 | async-start | bytes 12976128 | tf_op jit(solution)/shard_map/all_gather | solution.py:43
  9.3 527.5 %reduce-scatter.4.cloned.1.call-start = ((), (), s32[]{:S(2)}) async-start(), calls=%async_computation.7 | async-start | bytes 1572864 | tf_op jit(solution)/shard_map/reduce_scatter | solution.py:31
  187.4 327.2 %copy-start.4 = (bf16[256,2048]{1,0:T(8,128)(2,1)S(1)}, bf16[256,2048]{1,0:T(8,128)(2,1)}, u32[]{:S(2)}) copy-start(bf16[256,2048]{1,0:T(8,128)(2,1)} %all-gather.11.cloned.1.call-done) | copy-start | bytes 3145732
  196.9 343.7 %copy-start.2 = (bf16[256,1024]{1,0:T(8,128)(2,1)S(1)}, bf16[256,1024]{1,0:T(8,128)(2,1)}, u32[]{:S(2)}) copy-start(bf16[256,1024]{1,0:T(8,128)(2,1)} %param.10) | copy-start | bytes 1572868
  530.2 22.9 %all-gather.19.cloned.1.call-start = ((), (), s32[]{:S(2)}) async-start(), calls=%async_computation.8 | async-start | bytes 1572864 | tf_op jit(solution)/shard_map/all_gather | solution.py:25
  542.7 62.8 %all-gather.23.cloned.1.call-start = ((), (), s32[]{:S(2)}) async-start(), calls=%async_computation.10 | async-start | bytes 2359296 | tf_op jit(solution)/shard_map/all_gather | solution.py:63
  543.5 111.8 %all-gather.25.cloned.1.call-start = ((), (), s32[]{:S(2)}) async-start(), calls=%async_computation.11 | async-start | bytes 2359296 | tf_op jit(solution)/shard_map/all_gather | solution.py:61
  544.2 160.8 %all-gather.21.cloned.1.call-start = ((), (), s32[]{:S(2)}) async-start(), calls=%async_computation.9 | async-start | bytes 2359296 | tf_op jit(solution)/shard_map/all_gather | solution.py:62
  545.0 210.9 %all-gather.27.cloned.1.call-start = ((), (), s32[]{:S(2)}) async-start(), calls=%async_computation.12 | async-start | bytes 2359296 | tf_op jit(solution)/shard_map/all_gather | solution.py:72
  545.6 221.8 %reduce-scatter.6.cloned.1.call-start = ((), (), s32[]{:S(2)}) async-start(), calls=%async_computation.13 | async-start | bytes 1572864 | tf_op jit(solution)/shard_map/reduce_scatter | solution.py:31
  605.5 49.8 %copy-start.3 = (bf16[256,2048]{1,0:T(8,128)(2,1)S(1)}, bf16[256,2048]{1,0:T(8,128)(2,1)}, u32[]{:S(2)}) copy-start(bf16[256,2048]{1,0:T(8,128)(2,1)} %all-gather.19.cloned.1.call-done) | copy-start | bytes 3145732
  608.3 51.9 %copy-start.7 = (f32[3,512]{1,0:T(4,128)S(1)}, f32[3,512]{1,0:T(4,128)}, u32[]{:S(2)}) copy-start(f32[3,512]{1,0:T(4,128)} %param.18) | copy-start | bytes 18436
  657.6 98.2 %collective-permute-start = (f32[2,512]{1,0:T(2,128)S(1)}, f32[2,512]{1,0:T(2,128)S(1)}, u32[]{:S(2)}, u32[]{:S(2)}) collective-permute-start(f32[2,512]{1,0:T(2,128)S(1)} %slice.48), channel_id=1, source_target_pairs={{0,2},{2,4},{4,6},{6,8},{8,10},{10,12},{12,14},{1,3},{3,5},{5,7},{... | collective-permute-start | bytes 12296 | tf_op jit(solution)/shard_map/ppermute | solution.py:13
  755.9 15.1 %copy-start = (bf16[256,1024]{1,0:T(8,128)(2,1)S(1)}, bf16[256,1024]{1,0:T(8,128)(2,1)}, u32[]{:S(2)}) copy-start(bf16[256,1024]{1,0:T(8,128)(2,1)} %fusion.15) | copy-start | bytes 1572868
  760.6 22.9 %all-gather.29.cloned.1.call-start = ((), (), s32[]{:S(2)}) async-start(), calls=%async_computation.14 | async-start | bytes 1572864 | tf_op jit(solution)/shard_map/all_gather | solution.py:25
  773.1 46.8 %reduce-scatter.8.cloned.1.call-start = ((), (), s32[]{:S(2)}) async-start(), calls=%async_computation.15 | async-start | bytes 1572864 | tf_op jit(solution)/shard_map/reduce_scatter | solution.py:31
  785.0 9.5 %copy-start.5 = (bf16[256,2048]{1,0:T(8,128)(2,1)S(1)}, bf16[256,2048]{1,0:T(8,128)(2,1)}, u32[]{:S(2)}) copy-start(bf16[256,2048]{1,0:T(8,128)(2,1)} %all-gather.29.cloned.1.call-done) | copy-start | bytes 3145732
  794.5 29.1 %copy-start.1 = (bf16[256,1024]{1,0:T(8,128)(2,1)S(1)}, bf16[256,1024]{1,0:T(8,128)(2,1)}, u32[]{:S(2)}) copy-start(bf16[256,1024]{1,0:T(8,128)(2,1)} %fusion.19) | copy-start | bytes 1572868
Sparse Core Ops, SparseCore 0:
  8.9 11.7 all-gather.10
  22.8 164.4 all-gather.12
  189.6 161.4 all-gather.14
  353.0 161.4 all-gather.16
  530.3 6.5 reduce-scatter.3
  542.8 10.1 all-gather.18
  555.2 50.2 all-gather.22
  607.6 47.6 all-gather.24
  657.4 47.6 all-gather.20
  706.9 48.8 all-gather.26
  760.7 6.5 reduce-scatter.5
  773.2 10.1 all-gather.28
  810.4 9.5 reduce-scatter.7
where the time goes:
time: 833 us; the launch traced here: 832 us
  waiting for transfers between devices  734 us (88%)
  matrix products  60.1 us (7%)
  other arithmetic  14.6 us (2%)
  between operations  13.4 us (2%)
    all_gather x1, waiting for transfers between devices, shards(): lax.all_gather(w_gate, 'fs', axis=0, tiled=True)  165 us
    all_gather x1, waiting for transfers between devices, shards(): lax.all_gather(w_down, 'fs', axis=1, tiled=True)  163 us
    all_gather x1, waiting for transfers between devices, shards(): lax.all_gather(w_up, 'fs', axis=0, tiled=True)  154 us
    all_gather x1, waiting for transfers between devices, shards(): cgate = fold_rows(lax.all_gather(w_cgate, 'fs', axis=0, tiled=True))  50.9 us
    all_gather x1, waiting for transfers between devices, shards(): lax.all_gather(w_out, 'fs', axis=1, tiled=True)  50.8 us
    all_gather x1, waiting for transfers between devices, shards(): inner = fold_rows(lax.all_gather(w_inner, 'fs', axis=0, tiled=True))  47 us
    all_gather x1, waiting for transfers between devices, shards(): bgate = fold_rows(lax.all_gather(w_bgate, 'fs', axis=0, tiled=True))  44.9 us
    dot_general x2, matrix products, feed_forward(): partials = jnp.dot(hidden, down_whole, preferred_element_type=jnp.float32)  31.3 us
  transfers between devices with their start and end apart: 14, of which 13 were waited for; matrix products, arithmetic and copies ran while one was open for 2% of the time, Pallas kernels for 0%

commit v1 on v0

--- a/solution.py
+++ b/solution.py
@@ -5,6 +5,11 @@
 
 TAPS = 3
 EPSILON = 1e-06
+
+
+def gather_blocks(x, axis, dim):
+    tiles = lax.all_gather(x, axis)
+    return jnp.concatenate(tiles, axis=dim)
 
 
 def from_behind(x, axis, by):
@@ -68,9 +73,7 @@
     for tap in range(1, TAPS):
         conv = conv + conv_taps[tap] * padded[tap : tap + local_rows]
     gated = (bgate * conv).astype(jnp.bfloat16)
-    mix_partials = jnp.dot(
-        gated, lax.all_gather(w_out, "fs", axis=1, tiled=True), preferred_element_type=jnp.float32
-    )
+    mix_partials = jnp.dot(gated, gather_blocks(w_out, "fs", 1), preferred_element_type=jnp.float32)
     second = settle(first, mix_partials, 3, 1.0)
     return feed_forward(second, 4, 5)
 

time: 833 us -> 832 us (level)
  no operation moved by 1% of the time
where the time goes in v1:
time: 832 us; the launch traced here: 831 us
  waiting for transfers between devices  730 us (88%)
  matrix products  59.9 us (7%)
  other arithmetic  14.6 us (2%)
  between operations  13.4 us (2%)
    all_gather x1, waiting for transfers between devices, shards(): lax.all_gather(w_gate, 'fs', axis=0, tiled=True)  165 us
    all_gather x1, waiting for transfers between devices, shards(): lax.all_gather(w_down, 'fs', axis=1, tiled=True)  163 us
    all_gather x1, waiting for transfers between devices, shards(): lax.all_gather(w_up, 'fs', axis=0, tiled=True)  154 us
    all_gather x1, waiting for transfers between devices, shards(): cgate = fold_rows(lax.all_gather(w_cgate, 'fs', axis=0, tiled=True))  50.9 us
    all_gather x1, waiting for transfers between devices, shards(): inner = fold_rows(lax.all_gather(w_inner, 'fs', axis=0, tiled=True))  47 us
    all_gather x1, waiting for transfers between devices, shards(): bgate = fold_rows(lax.all_gather(w_bgate, 'fs', axis=0, tiled=True))  46.8 us
    all_gather x1, waiting for transfers between devices, gather_blocks(): tiles = lax.all_gather(x, axis)  44.9 us
    dot_general x2, matrix products, feed_forward(): partials = jnp.dot(hidden, down_whole, preferred_element_type=jnp.float32)  31.3 us
  transfers between devices with their start and end apart: 14, of which 13 were waited for; matrix products, arithmetic and copies ran while one was open for 2% of the time, Pallas kernels for 0%

profile of v1, /device:TPU:0, one launch (start us, length us, event | category | flops | bytes accessed | tf_op | source)
XLA Modules:
  0.0 831.2 jit_solution(13158161976948752682)
XLA Ops:
  6.5 0.0 all-gather.12.cloned.1.call-start
  6.5 0.7 all-gather.12.cloned.1.call-update
  7.3 0.0 all-gather.14.cloned.1.call-start
  7.3 0.7 all-gather.14.cloned.1.call-update
  8.0 0.0 all-gather.16.cloned.1.call-start
  8.1 0.7 all-gather.16.cloned.1.call-update
  8.8 0.0 all-gather.18.cloned.1.call-start
  8.8 0.5 all-gather.18.cloned.1.call-update
  9.3 0.0 reduce-scatter.4.cloned.1.call-start
  9.4 11.2 %all-gather.12.cloned.1.call-done = bf16[256,2048]{1,0:T(8,128)(2,1)} async-done(((bf16[256,1024]{1,0:T(8,128)(2,1)}), bf16[256,2048]{1,0:T(8,128)(2,1)}) %all-gather.12.cloned.1.call-update) | async-done | bytes 1048592 | tf_op jit(solution)/shard_map/all_gather | solution.py:30
  20.7 1.5 fusion.2
  22.2 165.2 %all-gather.14.cloned.1.call-done = bf16[2048,2816]{1,0:T(8,128)(2,1)} async-done(((bf16[256,2816]{1,0:T(8,128)(2,1)}), bf16[2048,2816]{1,0:T(8,128)(2,1)}) %all-gather.14.cloned.1.call-update) | async-done | bytes 11534352 | tf_op jit(solution)/shard_map/all_gather | solution.py:46
  187.4 9.5 %fusion.38 = f32[256,2816]{1,0:T(8,128)} fusion(bf16[2048,2816]{1,0:T(8,128)(2,1)} %all-gather.14.cloned.1.call-done, bf16[256,2048]{1,0:T(8,128)(2,1)} %all-gather.12.cloned.1.call-done, f32[2048]{0:T(1024)S(1)} %bitcast.33, f32[256]{0:T(256)S(1)} %add_rsqrt_fusion.5), kind=kOutput, calls=%fused_computation.54 | convolution fusion | flops 2954887168 | bytes 15475712 | tf_op jit(solution)/shard_map/dot_general | solution.py:53
  196.9 154.2 %all-gather.16.cloned.1.call-done = bf16[2048,2816]{1,0:T(8,128)(2,1)} async-done(((bf16[256,2816]{1,0:T(8,128)(2,1)}), bf16[2048,2816]{1,0:T(8,128)(2,1)}) %all-gather.16.cloned.1.call-update) | async-done | bytes 11534352 | tf_op jit(solution)/shard_map/all_gather | solution.py:47
  351.1 163.4 %all-gather.18.cloned.1.call-done = bf16[2816,2048]{1,0:T(8,128)(2,1)} async-done(((bf16[2816,256]{1,0:T(8,128)(2,1)}), bf16[2816,2048]{1,0:T(8,128)(2,1)}) %all-gather.18.cloned.1.call-update) | async-done | bytes 11534352 | tf_op jit(solution)/shard_map/all_gather | solution.py:48
  514.5 15.6 %convolution_convert_fusion.2 = bf16[256,2048]{1,0:T(8,128)(2,1)} fusion(bf16[2816,2048]{1,0:T(8,128)(2,1)} %all-gather.18.cloned.1.call-done, bf16[2048,2816]{1,0:T(8,128)(2,1)} %all-gather.16.cloned.1.call-done, f32[256,2816]{1,0:T(8,128)} %fusion.38, bf16[256,2048]{1,0:T(8,128)(2,1)S(1)} %copy-done.4, f32[2048]{0:T(1024)S(1)} %bitcast.34, ...), kind=kOutput, calls=%fused_computation.12 | convolution fusion | flops 5912526848 | bytes 28058624 | tf_op jit(solution)/shard_map/dot_general | solution.py:56
  530.1 0.0 reduce-scatter.4.cloned.1.call-update
  530.2 0.0 all-gather.20.cloned.1.call-start
  530.2 6.6 reduce-scatter.4.cloned.1.call-done
  536.9 1.2 fusion.11
  538.1 2.5 psum.21
  540.6 0.0 copy-done.2
  540.6 2.1 fusion.15
  542.7 0.0 all-gather.20.cloned.1.call-update
  542.7 0.0 all-gather.24.cloned.1.call-start
  542.8 0.7 all-gather.24.cloned.1.call-update
  543.5 0.0 all-gather.26.cloned.1.call-start
  543.5 0.7 all-gather.26.cloned.1.call-update
  544.2 0.0 all-gather.30.cloned.1.call-start
  544.3 0.7 all-gather.30.cloned.1.call-update
  545.0 0.0 all-gather.22.cloned.1.call-start
  545.0 0.5 all-gather.22.cloned.1.call-update
  545.6 0.0 reduce-scatter.6.cloned.1.call-start
  545.6 7.5 all-gather.20.cloned.1.call-done
  553.1 1.5 fusion.5
  554.6 50.9 %all-gather.24.cloned.1.call-done = bf16[2048,512]{1,0:T(8,128)(2,1)} async-done(((bf16[256,512]{1,0:T(8,128)(2,1)}), bf16[2048,512]{1,0:T(8,128)(2,1)}) %all-gather.24.cloned.1.call-update) | async-done | bytes 2097168 | tf_op jit(solution)/shard_map/all_gather | solution.py:68
  605.5 2.7 fusion.48
  608.3 0.0 copy-start.7
  608.3 47.0 %all-gather.26.cloned.1.call-done = bf16[2048,512]{1,0:T(8,128)(2,1)} async-done(((bf16[256,512]{1,0:T(8,128)(2,1)}), bf16[2048,512]{1,0:T(8,128)(2,1)}) %all-gather.26.cloned.1.call-update) | async-done | bytes 2097168 | tf_op jit(solution)/shard_map/all_gather | solution.py:66
  655.3 2.3 convolution_multiply_fusion.2
  657.6 2.5 collective-permute-start
  660.1 44.9 %all-gather.30.cloned.1.call-done = bf16[4096,256]{1,0:T(8,128)(2,1)} async-done(((bf16[512,256]{1,0:T(8,128)(2,1)}), bf16[4096,256]{1,0:T(8,128)(2,1)}) %all-gather.30.cloned.1.call-update) | async-done | bytes 2097168 | tf_op jit(solution)/shard_map/all_gather | solution.py:11
  705.1 2.9 copy.11
  707.9 46.8 %all-gather.22.cloned.1.call-done = bf16[2048,512]{1,0:T(8,128)(2,1)} async-done(((bf16[256,512]{1,0:T(8,128)(2,1)}), bf16[2048,512]{1,0:T(8,128)(2,1)}) %all-gather.22.cloned.1.call-update) | async-done | bytes 2097168 | tf_op jit(solution)/shard_map/all_gather | solution.py:67
  754.7 0.0 collective-permute-done
  754.7 4.4 convolution_convert_fusion.1
  759.1 0.0 reduce-scatter.6.cloned.1.call-update
  759.2 0.0 all-gather.28.cloned.1.call-start
  759.2 7.0 reduce-scatter.6.cloned.1.call-done
  766.2 1.2 fusion.16
  767.4 2.5 psum.22
  769.9 2.1 fusion.19
  772.0 0.0 all-gather.28.cloned.1.call-update
  772.0 0.2 reduce-scatter.8.cloned.1.call-start
  772.3 10.1 %all-gather.28.cloned.1.call-done = bf16[256,2048]{1,0:T(8,128)(2,1)} async-done(((bf16[256,1024]{1,0:T(8,128)(2,1)}), bf16[256,2048]{1,0:T(8,128)(2,1)}) %all-gather.28.cloned.1.call-update) | async-done | bytes 1048592 | tf_op jit(solution)/shard_map/all_gather | solution.py:30
  782.4 1.5 fusion.8
  783.9 0.0 copy-start.5
  783.9 9.5 %fusion.34 = f32[256,2816]{1,0:T(8,128)} fusion(bf16[2048,2816]{1,0:T(8,128)(2,1)} %all-gather.14.cloned.1.call-done, bf16[256,2048]{1,0:T(8,128)(2,1)} %all-gather.28.cloned.1.call-done, f32[2048]{0:T(1024)S(1)} %bitcast.28, f32[256]{0:T(256)S(1)} %add_rsqrt_fusion.1), kind=kOutput, calls=%fused_computation.53 | convolution fusion | flops 2954887168 | bytes 15475712 | tf_op jit(solution)/shard_map/dot_general | solution.py:53
  793.4 15.7 %convolution_convert_fusion = bf16[256,2048]{1,0:T(8,128)(2,1)} fusion(bf16[2816,2048]{1,0:T(8,128)(2,1)} %all-gather.18.cloned.1.call-done, bf16[2048,2816]{1,0:T(8,128)(2,1)} %all-gather.16.cloned.1.call-done, f32[256,2816]{1,0:T(8,128)} %fusion.34, bf16[256,2048]{1,0:T(8,128)(2,1)S(1)} %copy-done.5, f32[2048]{0:T(1024)S(1)} %bitcast.29, ...), kind=kOutput, calls=%fused_computation.10 | convolution fusion | flops 5912526848 | bytes 28058624 | tf_op jit(solution)/shard_map/dot_general | solution.py:56
  809.1 0.0 reduce-scatter.8.cloned.1.call-update
  809.2 9.7 %reduce-scatter.8.cloned.1.call-done = bf16[256,1024]{1,0:T(8,128)(2,1)} async-done(((bf16[256,2048]{1,0:T(8,128)(2,1)}), bf16[256,1024]{1,0:T(8,128)(2,1)}) %reduce-scatter.8.cloned.1.call-update) | async-done | bytes 524304 | tf_op jit(solution)/shard_map/reduce_scatter | solution.py:36
  818.9 1.2 fusion.20
  820.1 2.5 psum.23
  822.6 2.1 fusion.24
  (25 shorter events, 0.2 us)
Async XLA Ops:
  6.5 14.1 %all-gather.12.cloned.1.call-start = ((), (), s32[]{:S(2)}) async-start(), calls=%async_computation.3 | async-start | bytes 1572864 | tf_op jit(solution)/shard_map/all_gather | solution.py:30
  7.3 2.1 copy-start.6
  7.3 180.1 %all-gather.14.cloned.1.call-start = ((), (), s32[]{:S(2)}) async-start(), calls=%async_computation.4 | async-start | bytes 12976128 | tf_op jit(solution)/shard_map/all_gather | solution.py:46
  8.0 343.1 %all-gather.16.cloned.1.call-start = ((), (), s32[]{:S(2)}) async-start(), calls=%async_computation.5 | async-start | bytes 12976128 | tf_op jit(solution)/shard_map/all_gather | solution.py:47
  8.8 505.8 %all-gather.18.cloned.1.call-start = ((), (), s32[]{:S(2)}) async-start(), calls=%async_computation.6 | async-start | bytes 12976128 | tf_op jit(solution)/shard_map/all_gather | solution.py:48
  9.3 527.5 %reduce-scatter.4.cloned.1.call-start = ((), (), s32[]{:S(2)}) async-start(), calls=%async_computation.7 | async-start | bytes 1572864 | tf_op jit(solution)/shard_map/reduce_scatter | solution.py:36
  187.4 327.2 %copy-start.4 = (bf16[256,2048]{1,0:T(8,128)(2,1)S(1)}, bf16[256,2048]{1,0:T(8,128)(2,1)}, u32[]{:S(2)}) copy-start(bf16[256,2048]{1,0:T(8,128)(2,1)} %all-gather.12.cloned.1.call-done) | copy-start | bytes 3145732
  196.9 343.7 %copy-start.2 = (bf16[256,1024]{1,0:T(8,128)(2,1)S(1)}, bf16[256,1024]{1,0:T(8,128)(2,1)}, u32[]{:S(2)}) copy-start(bf16[256,1024]{1,0:T(8,128)(2,1)} %param.10) | copy-start | bytes 1572868
  530.2 22.9 %all-gather.20.cloned.1.call-start = ((), (), s32[]{:S(2)}) async-start(), calls=%async_computation.8 | async-start | bytes 1572864 | tf_op jit(solution)/shard_map/all_gather | solution.py:30
  542.7 62.8 %all-gather.24.cloned.1.call-start = ((), (), s32[]{:S(2)}) async-start(), calls=%async_computation.10 | async-start | bytes 2359296 | tf_op jit(solution)/shard_map/all_gather | solution.py:68
  543.5 111.8 %all-gather.26.cloned.1.call-start = ((), (), s32[]{:S(2)}) async-start(), calls=%async_computation.11 | async-start | bytes 2359296 | tf_op jit(solution)/shard_map/all_gather | solution.py:66
  544.2 160.8 %all-gather.30.cloned.1.call-start = ((), (), s32[]{:S(2)}) async-start(), calls=%async_computation.15 | async-start | bytes 2359296 | tf_op jit(solution)/shard_map/all_gather | solution.py:11
  545.0 209.7 %all-gather.22.cloned.1.call-start = ((), (), s32[]{:S(2)}) async-start(), calls=%async_computation.9 | async-start | bytes 2359296 | tf_op jit(solution)/shard_map/all_gather | solution.py:67
  545.6 220.7 %reduce-scatter.6.cloned.1.call-start = ((), (), s32[]{:S(2)}) async-start(), calls=%async_computation.12 | async-start | bytes 1572864 | tf_op jit(solution)/shard_map/reduce_scatter | solution.py:36
  605.5 49.8 %copy-start.3 = (bf16[256,2048]{1,0:T(8,128)(2,1)S(1)}, bf16[256,2048]{1,0:T(8,128)(2,1)}, u32[]{:S(2)}) copy-start(bf16[256,2048]{1,0:T(8,128)(2,1)} %all-gather.20.cloned.1.call-done) | copy-start | bytes 3145732
  608.3 51.9 %copy-start.7 = (f32[3,512]{1,0:T(4,128)S(1)}, f32[3,512]{1,0:T(4,128)}, u32[]{:S(2)}) copy-start(f32[3,512]{1,0:T(4,128)} %param.18) | copy-start | bytes 18436
  657.6 97.1 %collective-permute-start = (f32[2,512]{1,0:T(2,128)S(1)}, f32[2,512]{1,0:T(2,128)S(1)}, u32[]{:S(2)}, u32[]{:S(2)}) collective-permute-start(f32[2,512]{1,0:T(2,128)S(1)} %slice.48), channel_id=1, source_target_pairs={{0,2},{2,4},{4,6},{6,8},{8,10},{10,12},{12,14},{1,3},{3,5},{5,7},{... | collective-permute-start | bytes 12296 | tf_op jit(solution)/shard_map/ppermute | solution.py:18
  754.7 15.2 %copy-start = (bf16[256,1024]{1,0:T(8,128)(2,1)S(1)}, bf16[256,1024]{1,0:T(8,128)(2,1)}, u32[]{:S(2)}) copy-start(bf16[256,1024]{1,0:T(8,128)(2,1)} %fusion.15) | copy-start | bytes 1572868
  759.2 23.2 %all-gather.28.cloned.1.call-start = ((), (), s32[]{:S(2)}) async-start(), calls=%async_computation.13 | async-start | bytes 1572864 | tf_op jit(solution)/shard_map/all_gather | solution.py:30
  772.0 46.8 %reduce-scatter.8.cloned.1.call-start = ((), (), s32[]{:S(2)}) async-start(), calls=%async_computation.14 | async-start | bytes 1572864 | tf_op jit(solution)/shard_map/reduce_scatter | solution.py:36
  783.9 9.5 %copy-start.5 = (bf16[256,2048]{1,0:T(8,128)(2,1)S(1)}, bf16[256,2048]{1,0:T(8,128)(2,1)}, u32[]{:S(2)}) copy-start(bf16[256,2048]{1,0:T(8,128)(2,1)} %all-gather.28.cloned.1.call-done) | copy-start | bytes 3145732
  793.4 29.1 %copy-start.1 = (bf16[256,1024]{1,0:T(8,128)(2,1)S(1)}, bf16[256,1024]{1,0:T(8,128)(2,1)}, u32[]{:S(2)}) copy-start(bf16[256,1024]{1,0:T(8,128)(2,1)} %fusion.19) | copy-start | bytes 1572868
Sparse Core Ops, SparseCore 0:
  8.9 11.7 all-gather.11
  22.8 164.4 all-gather.13
  189.6 161.4 all-gather.15
  353.0 161.4 all-gather.17
  530.3 6.5 reduce-scatter.3
  542.8 10.1 all-gather.19
  555.2 50.2 all-gather.23
  607.6 47.6 all-gather.25
  657.4 47.6 all-gather.29
  707.0 47.6 all-gather.21
  759.3 6.9 reduce-scatter.5
  772.2 10.1 all-gather.27
  809.3 9.5 reduce-scatter.7
